TPU v7x, 32 devices: a whole 2x2x4 slice. The times are simulated.
32 devices in a mesh: sp: 4 (over x, core), tp: 8 (over z, y).
Axes of the slice: x: 2, y: 2, z: 4, core: 2. Of those that a mesh axis runs over, the one named last changes fastest.
Arguments:
- latent: bfloat16 [512, 4096], P('sp', 'tp'), may hold values from -60 to 60
- context: bfloat16 [64, 4096], P('sp', 'tp'), may hold values from -6 to 6
- conditioning: bfloat16 [4096], P('sp'), may hold values from -6 to 6
- context_prompt_vector: bfloat16 [4096], P('sp'), may hold values from -6 to 6
- shift_matrix: bfloat16 [4096, 4096], P('tp', 'sp'), may hold values from -0.09375 to 0.09375
- scale_matrix: bfloat16 [4096, 4096], P('tp', 'sp'), may hold values from -0.09375 to 0.09375
- residual_gate_matrix: bfloat16 [4096, 4096], P('tp', 'sp'), may hold values from -0.09375 to 0.09375
- query_matrix: bfloat16 [2048, 4096], P('tp'), may hold values from -0.09375 to 0.09375
- key_matrix: bfloat16 [2048, 4096], P('tp'), may hold values from -0.09375 to 0.09375
- value_matrix: bfloat16 [4096, 4096], P('tp'), may hold values from -0.09375 to 0.09375
- gate_matrix: bfloat16 [4096, 4096], P('tp'), may hold values from -0.09375 to 0.09375
- decay_down_factor: bfloat16 [2, 4096, 16], replicated, may hold values from -0.09375 to 0.09375
- decay_up_factor: bfloat16 [2, 16, 2048], replicated, may hold values from -1.5 to 1.5
- decay_key_bias: float32 [2, 2048], replicated, may hold values from -0.5 to 7
- spike_log_decay: float32 [2, 512, 16], P(None, 'sp'), may hold values from -2.8 to 0
- output_gain: float32 [4096], P('tp'), may hold values from 0.1 to 1.9
- output_matrix: bfloat16 [4096, 4096], P('tp'), may hold values from -0.375 to 0.375
Outputs:
- mixed: bfloat16 [512, 4096], P('sp', 'tp')
All inputs are finite; a program needn't handle non-finite values.
Results may differ from a plain program's by a relative error of at most 0.013.
Values may be sent and summed in bfloat16 or wider, within the bound.
A program may use at most 64 MiB of HBM per device.

v0:
```python
import jax
import jax.numpy as jnp
from jax import lax
from jax.sharding import PartitionSpec as P

D = 4096
HEADS = 16
DK = 128
DECAY_RANK = 16
BLK = 64
VGROUP = 64


epsilon = 1e-05
gate_norm = 16.0
precise = lax.Precision.HIGHEST


def for_sending(value):

    def short(part):
        return part.astype(jnp.bfloat16) if part.dtype == jnp.float32 else part

    return jax.tree.map(short, value)


def from_partner(value, axis, distance):
    return lax.ppermute(value, axis, [(i, i ^ 1 << distance) for i in range(lax.axis_size(axis))])


def carried_in(value, axis, combine, identity, reverse):
    peers, index = (lax.axis_size(axis), lax.axis_index(axis))
    everything = jax.tree.map(
        lambda part, kind: lax.all_gather(part.astype(kind), axis),
        value,
        (jnp.bfloat16, jnp.bfloat16),
    )
    start = jax.tree.map(
        lambda part, zero: jnp.broadcast_to(jnp.asarray(zero, part.dtype), part.shape),
        value,
        identity,
    )

    def turn(k, before):
        at = peers - 1 - k if reverse else k
        reached = at > index if reverse else at < index
        new = combine(
            before, jax.tree.map(lambda part, own: part[at].astype(own.dtype), everything, value)
        )
        return jax.tree.map(lambda a, b: jnp.where(reached, a, b), new, before)

    return lax.fori_loop(0, peers, turn, start)


def linear(rows, weight):
    return lax.dot_general(
        rows, weight, (((1,), (1,)), ((), ())), preferred_element_type=jnp.float32
    )


def modulated(rows, row_sum, row_squares, shift_vec, scale_vec):
    rows_f = rows.astype(jnp.float32)
    mean_val = row_sum / D
    variance = row_squares / D - mean_val * mean_val
    return (
        (rows_f - mean_val) * lax.rsqrt(variance + epsilon) * (1.0 + scale_vec) + shift_vec
    ).astype(jnp.bfloat16)


def reverse_rows(array):
    return jnp.flip(array, axis=0)


def end_state(key_rows, value_rows, log_decay):
    cumulative = jnp.cumsum(log_decay, axis=0)
    totals = cumulative[-1]
    weighted = key_rows * jnp.exp(totals - cumulative)
    return (jnp.exp(totals), jnp.einsum("nhd,nhe->hde", weighted, value_rows, precision=precise))


def combine(earlier, later):
    return (earlier[0] * later[0], later[0][..., None] * earlier[1] + later[1])


def blockwise(queries, key_rows, value_rows, log_decay, carried, block_len):
    length, head_count, _ = queries.shape
    value_width = value_rows.shape[-1]
    blocks = length // block_len

    def shaped(array):
        return array.reshape(blocks, block_len, head_count, array.shape[-1])

    triangle = jnp.tril(jnp.ones((block_len, block_len), jnp.float32))

    def advance(state_now, inputs):
        block_q, block_k, block_v, block_a = inputs
        cumulative = jnp.cumsum(block_a, axis=0)
        block_end = cumulative[-1]
        query_dec = block_q * jnp.exp(cumulative)
        scores = (
            jnp.einsum("ihd,jhd->hij", query_dec, block_k * jnp.exp(-cumulative), precision=precise)
            * triangle
        )
        result = jnp.einsum("hij,jhe->ihe", scores, block_v, precision=precise)
        result = result + jnp.einsum("ihd,hde->ihe", query_dec, state_now, precision=precise)
        state_next = state_now * jnp.exp(block_end)[:, :, None] + jnp.einsum(
            "jhd,jhe->hde", block_k * jnp.exp(block_end - cumulative), block_v, precision=precise
        )
        return (state_next, result)

    _, outputs = lax.scan(
        advance, carried, (shaped(queries), shaped(key_rows), shaped(value_rows), shaped(log_decay))
    )
    return outputs.reshape(length, head_count, value_width)


def head_channels(pieces, per_head, tp_index):
    for bit_number in range(per_head.bit_length() - 1):
        partner = from_partner(
            (for_sending(pieces[0]), for_sending(pieces[1]), for_sending(pieces[2])),
            "tp",
            bit_number,
        )
        upper = tp_index // (1 << bit_number) % 2 == 1
        pieces = tuple(
            (
                jnp.where(
                    upper,
                    jnp.concatenate([theirs, mine], axis=1),
                    jnp.concatenate([mine, theirs], axis=1),
                )
                for mine, theirs in zip(pieces, partner)
            )
        )
    return pieces


def context_totals(fwd_growth, fwd_state, bwd_growth, bwd_state, identity):

    def absorb(carried, piece):
        return (combine(carried, piece), None)

    total_fwd, _ = lax.scan(absorb, identity, (fwd_growth, fwd_state))
    total_bwd, _ = lax.scan(absorb, identity, (bwd_growth, bwd_state), reverse=True)
    return (total_fwd, total_bwd)


def stored(array):
    return lax.optimization_barrier(array.astype(jnp.bfloat16))


def local(
    latent,
    context,
    conditioning,
    context_prompt_vector,
    shift_matrix,
    scale_matrix,
    residual_gate_matrix,
    query_matrix,
    key_matrix,
    value_matrix,
    gate_matrix,
    decay_down_factor,
    decay_up_factor,
    decay_key_bias,
    spike_log_decay,
    output_gain,
    output_matrix,
):
    tp_count = lax.axis_size("tp")
    tp_index = lax.axis_index("tp")
    per_head = max(tp_count // HEADS, 1)
    heads_per_shard = max(HEADS // tp_count, 1)
    leading_head = tp_index // per_head * heads_per_shard
    tok_rows = latent.shape[0]
    conds = jax.nn.silu(
        jnp.stack([conditioning, context_prompt_vector]).astype(jnp.float32)
    ).astype(jnp.bfloat16)
    shifts, scales, gates = lax.psum(
        (
            linear(conds, shift_matrix),
            linear(conds, scale_matrix),
            linear(conds, residual_gate_matrix),
        ),
        "sp",
    )
    down_both = jnp.concatenate([decay_down_factor[0].T, decay_down_factor[1].T], axis=0)
    lat_weights = (query_matrix, key_matrix, value_matrix, gate_matrix, down_both)
    ctx_weights = (key_matrix, value_matrix, down_both)
    lat_f = latent.astype(jnp.float32)
    ctx_f = context.astype(jnp.float32)
    lat_sum, lat_squares, ctx_sum, ctx_squares = lax.psum(
        (
            jnp.sum(lat_f, axis=1, keepdims=True),
            jnp.sum(lat_f * lat_f, axis=1, keepdims=True),
            jnp.sum(ctx_f, axis=1, keepdims=True),
            jnp.sum(ctx_f * ctx_f, axis=1, keepdims=True),
        ),
        "tp",
    )
    latent_normalized = modulated(latent, lat_sum, lat_squares, shifts[0], scales[0])
    normed_ctx = modulated(context, ctx_sum, ctx_squares, shifts[1], scales[1])
    lat_piece = lax.all_gather(latent_normalized, "tp", axis=1, tiled=True)
    ctx_piece = lax.all_gather(normed_ctx, "tp", axis=1, tiled=True)
    lat_new = tuple((linear(lat_piece, weight) for weight in lat_weights))
    ctx_new = tuple((linear(ctx_piece, weight) for weight in ctx_weights))
    query_part, key_part, value_part, gate_part, low_rank_part = lat_new
    ctx_key_part, ctx_value_part, ctx_low = ctx_new
    query_full, key_full, ctx_key_full = head_channels(
        (stored(query_part), stored(key_part), stored(ctx_key_part)), per_head, tp_index
    )

    def split_heads(rows, width):
        return rows.astype(jnp.float32).reshape(rows.shape[0], heads_per_shard, width)

    value_cols = value_part.shape[1] // heads_per_shard
    queries = split_heads(query_full, DK) * DK ** (-0.5)
    key_rows = split_heads(key_full, DK)
    ctx_keys = split_heads(ctx_key_full, DK)
    values_lat = split_heads(stored(value_part), value_cols)
    values_ctx = split_heads(stored(ctx_value_part), value_cols)
    gate_rows = stored(gate_part).astype(jnp.float32)

    def per_head_decay(low_rows, direction):
        up_part = lax.dynamic_slice_in_dim(
            decay_up_factor[direction], leading_head * DK, heads_per_shard * DK, 1
        ).astype(jnp.float32)
        bias_part = lax.dynamic_slice_in_dim(
            decay_key_bias[direction], leading_head * DK, heads_per_shard * DK, 0
        )
        pre_act = jnp.dot(low_rows, up_part, precision=precise) + bias_part
        return (jax.nn.log_sigmoid(pre_act) / gate_norm).reshape(
            low_rows.shape[0], heads_per_shard, DK
        )

    decay_spikes = lax.dynamic_slice_in_dim(spike_log_decay, leading_head, heads_per_shard, 2)
    latent_forward = per_head_decay(low_rank_part[:, :DECAY_RANK], 0) + decay_spikes[0][:, :, None]
    latent_backward = per_head_decay(low_rank_part[:, DECAY_RANK:], 1) + decay_spikes[1][:, :, None]
    ctx_fwd = per_head_decay(ctx_low[:, :DECAY_RANK], 0)
    ctx_bwd = per_head_decay(ctx_low[:, DECAY_RANK:], 1)
    cf_growth, cf_state = end_state(ctx_keys, values_ctx, ctx_fwd)
    cb_growth, cb_state = end_state(
        reverse_rows(ctx_keys), reverse_rows(values_ctx), reverse_rows(ctx_bwd)
    )
    lf_growth, lf_state = end_state(key_rows, values_lat, latent_forward)
    lb_growth, lb_state = end_state(
        reverse_rows(key_rows), reverse_rows(values_lat), reverse_rows(latent_backward)
    )
    identity = (
        jnp.ones((heads_per_shard, DK), jnp.float32),
        jnp.zeros((heads_per_shard, DK, value_cols), jnp.float32),
    )
    ctx_gathered = (
        lax.all_gather(cf_growth[None].astype(jnp.bfloat16), "sp", axis=0, tiled=True).astype(
            jnp.float32
        ),
        lax.all_gather(cf_state[None].astype(jnp.bfloat16), "sp", axis=0, tiled=True).astype(
            jnp.float32
        ),
        lax.all_gather(cb_growth[None].astype(jnp.bfloat16), "sp", axis=0, tiled=True).astype(
            jnp.float32
        ),
        lax.all_gather(cb_state[None].astype(jnp.bfloat16), "sp", axis=0, tiled=True).astype(
            jnp.float32
        ),
    )
    total_fwd, total_bwd = context_totals(
        ctx_gathered[0], ctx_gathered[1], ctx_gathered[2], ctx_gathered[3], identity
    )
    prefix = carried_in((lf_growth, lf_state), "sp", combine, identity, False)
    suffix = carried_in((lb_growth, lb_state), "sp", combine, identity, True)
    start_fwd = combine(total_fwd, prefix)[1]
    start_bwd = combine(total_bwd, suffix)[1]
    zero_state = jnp.zeros((heads_per_shard, DK, value_cols), jnp.float32)

    def direction_out(query_rows, key_list, value_list, log_decay, start_state):
        local_part = blockwise(query_rows, key_list, value_list, log_decay, zero_state, BLK)
        reach = query_rows * jnp.exp(jnp.cumsum(log_decay, axis=0))
        return local_part + jnp.einsum("nhd,hde->nhe", reach, start_state, precision=precise)

    out_fwd = direction_out(queries, key_rows, values_lat, latent_forward, start_fwd)
    out_bwd = reverse_rows(
        direction_out(
            reverse_rows(queries),
            reverse_rows(key_rows),
            reverse_rows(values_lat),
            reverse_rows(latent_backward),
            start_bwd,
        )
    )
    grouped = (out_fwd + out_bwd).reshape(tok_rows, -1, VGROUP)
    grouped = grouped * lax.rsqrt(jnp.mean(grouped * grouped, axis=-1, keepdims=True) + epsilon)
    heads_out = (grouped.reshape(tok_rows, -1) * output_gain * jax.nn.silu(gate_rows)).astype(
        jnp.bfloat16
    )
    branch = linear(lax.all_gather(heads_out, "tp", axis=1, tiled=True), output_matrix)
    return (latent.astype(jnp.float32) + gates[0] * branch).astype(jnp.bfloat16)


def solution(mesh):
    placed = (
        P("sp", "tp"),
        P("sp", "tp"),
        P("sp"),
        P("sp"),
        P("tp", "sp"),
        P("tp", "sp"),
        P("tp", "sp"),
        P("tp", None),
        P("tp", None),
        P("tp", None),
        P("tp", None),
        P(),
        P(),
        P(),
        P(None, "sp", None),
        P("tp"),
        P("tp", None),
    )
    return jax.shard_map(
        local, mesh=mesh, in_specs=placed, out_specs=P("sp", "tp"), check_vma=False
    )
```

profile of v0, /device:TPU:0, one launch (start us, length us, event | category | flops | bytes accessed | tf_op | source)
XLA Modules:
  0.0 266.8 jit_solution(12194387579442730119)
XLA Ops:
  8.1 1.6 fusion.121
  9.7 1.6 fusion.123
  11.3 1.6 fusion.125
  12.9 1.0 convert_reduce_fusion
  14.8 13.2 %all-reduce.1 = (f32[2,512]{1,0:T(2,128)S(1)}, f32[2,512]{1,0:T(2,128)S(1)}, f32[2,512]{1,0:T(2,128)}) all-reduce(f32[2,512]{1,0:T(2,128)S(1)} %fusion.121, f32[2,512]{1,0:T(2,128)S(1)} %fusion.123, f32[2,512]{1,0:T(2,128)S(1)} %fusion.125), channel_id=1, replica_groups=mesh['sp'=4,'tp'=8] {'sp'}, use_global_device_ids=true, to_apply=%region_6.7 | all-reduce | flops 3072 | bytes 24576 | tf_op jit(solution)/shard_map/psum | solution.py:180
  28.0 21.7 %all-reduce = (f32[128,1]{0,1:T(1,128)S(1)}, f32[128,1]{0,1:T(1,128)S(1)}, f32[16,1]{0,1:T(1,128)S(1)}, f32[16,1]{0,1:T(1,128)S(1)}) all-reduce(f32[128,1]{0,1:T(1,128)S(1)} %bitcast.291, f32[128,1]{0,1:T(1,128)S(1)} %bitcast.290, f32[16,1]{0,1:T(1,128)S(1)} %bitcast.293, f32[16,1]{0,1:T(1,128)S(1)} %bitcast.292), channel_id=1, replica_groups=mesh['sp'=4,'tp'=8] {'tp'}, use_global_device_ids=true, to_apply=%region_4.5 | all-reduce | flops 288 | bytes 2304 | tf_op jit(solution)/shard_map/psum | solution.py:193
  49.7 1.7 fusion.62
  53.5 31.0 %all_gather.45 = bf16[16,4096]{1,0:T(8,128)(2,1)S(1)} all-gather(bf16[16,512]{1,0:T(8,128)(2,1)S(1)} %fusion.89), channel_id=1, replica_groups=mesh['sp'=4,'tp'=8] {'tp'}, dimensions={1}, use_global_device_ids=true | all-gather | bytes 147456 | tf_op jit(solution)/shard_map/all_gather | solution.py:205
  84.9 3.4 %convolution_convert_fusion.8 = bf16[16,512]{1,0:T(8,128)(2,1)S(1)} fusion(bf16[16,4096]{1,0:T(8,128)(2,1)S(1)} %all_gather.45, bf16[512,4096]{1,0:T(8,128)(2,1)} %param.38), kind=kOutput, calls=%fused_computation.96 | convolution fusion | flops 67117056 | bytes 4341760 | tf_op jit(solution)/shard_map/dot_general | solution.py:56
  89.8 5.1 %all_gather.46 = bf16[4,2,128]{2,1,0:T(2,128)(2,1)S(1)} all-gather(bf16[1,2,128]{2,1,0:T(2,128)(2,1)S(1)} %get-tuple-element.728), channel_id=1, replica_groups=mesh['sp'=4,'tp'=8] {'sp'}, dimensions={0}, use_global_device_ids=true | all-gather | bytes 2560 | tf_op jit(solution)/shard_map/all_gather | solution.py:255
  95.8 7.3 %all-gather.1 = bf16[8,128,256]{2,1,0:T(8,128)(2,1)S(1)} all-gather(bf16[2,128,256]{2,1,0:T(8,128)(2,1)S(1)} %convolution_convert_fusion.5), channel_id=3, replica_groups=mesh['sp'=4,'tp'=8] {'sp'}, dimensions={0}, use_global_device_ids=true | all-gather | bytes 655360 | tf_op jit(solution)/shard_map/all_gather | solution.py:258
  106.9 5.0 %all_gather.51 = bf16[4,2,128]{2,1,0:T(2,128)(2,1)S(1)} all-gather(bf16[1,2,128]{2,1,0:T(2,128)(2,1)S(1)} %get-tuple-element.734), channel_id=1, replica_groups=mesh['sp'=4,'tp'=8] {'sp'}, dimensions={0}, use_global_device_ids=true | all-gather | bytes 2560 | tf_op jit(solution)/shard_map/all_gather | solution.py:261
  112.7 1.1 convolution_convert_fusion.4
  113.8 7.5 %all-gather.3 = bf16[8,128,256]{2,1,0:T(8,128)(2,1)S(1)} all-gather(bf16[2,128,256]{2,1,0:T(8,128)(2,1)S(1)} %convolution_convert_fusion.4), channel_id=5, replica_groups=mesh['sp'=4,'tp'=8] {'sp'}, dimensions={0}, use_global_device_ids=true | all-gather | bytes 655360 | tf_op jit(solution)/shard_map/all_gather | solution.py:264
  121.3 1.1 convert.9
  122.4 4.4 %while.91 = (s32[]{:T(128)}, f32[2,128,256]{2,1,0:T(8,128)S(1)}, f32[4,2,128]{2,1,0:T(2,128)S(1)}, f32[4,2,128,256]{3,2,1,0:T(8,128)}, s32[]{:T(128)}, /*index=5*/s32[]{:T(128)}, s32[]{:T(128)}) while((s32[]{:T(128)}, f32[2,128,256]{2,1,0:T(8,128)S(1)}, f32[4,2,128]{2,1,0:T(2,128)S(1)}, f32[4,2,128,256]{3,2,1,0:T(8,128)}, ...), condition=%wide.region_28.29_spmd.clone, body=%wide.region_27.28_spmd.clone.sunk | while | flops 196612 | bytes 789619 | solution.py:144
  122.4 1.1 bitcast_add_fusion.5
  123.5 1.1 bitcast_add_fusion.5
  124.6 1.1 bitcast_add_fusion.5
  125.7 1.1 bitcast_add_fusion.5
  127.5 1.8 fusion.70
  129.3 1.7 fusion.74
  133.5 2.1 convolution_convert_fusion.7
  137.0 3.7 %convolution_convert_fusion.2 = bf16[128,512]{1,0:T(8,128)(2,1)S(1)} fusion(bf16[128,4096]{1,0:T(8,128)(2,1)S(1)} %copy-done.1, bf16[512,4096]{1,0:T(8,128)(2,1)} %param.38), kind=kOutput, calls=%fused_computation.85 | convolution fusion | flops 536936448 | bytes 5373952 | tf_op jit(solution)/shard_map/dot_general | solution.py:56
  142.3 3.1 %convolution_convert_fusion.6 = bf16[128,256]{1,0:T(8,128)(2,1)} fusion(bf16[128,4096]{1,0:T(8,128)(2,1)S(1)} %copy-done.1, bf16[256,4096]{1,0:T(8,128)(2,1)} %param.36), kind=kOutput, calls=%fused_computation.94 | convolution fusion | flops 268468224 | bytes 3211264 | tf_op jit(solution)/shard_map/dot_general | solution.py:56
  145.4 1.6 reshape.143
  146.9 1.5 broadcast_multiply_fusion
  148.4 4.4 %convolution_convert_fusion = bf16[128,512]{1,0:T(8,128)(2,1)} fusion(bf16[128,4096]{1,0:T(8,128)(2,1)S(1)} %copy-done.1, bf16[512,4096]{1,0:T(8,128)(2,1)} %param.39), kind=kOutput, calls=%fused_computation.83 | convolution fusion | flops 536936448 | bytes 5373952 | tf_op jit(solution)/shard_map/dot_general | solution.py:56
  153.8 1.0 broadcast_add_fusion
  157.7 1.1 fusion.83
  158.9 2.3 exponential_multiply_fusion.2
  161.9 5.9 %while.89 = (s32[]{:T(128)}, f32[2,128,256]{2,1,0:T(8,128)S(1)}, f32[2,64,2,256]{3,1,0,2:T(8,128)}, f32[2,64,2,128]{3,2,1,0:T(2,128)S(1)}, f32[2,64,2,128]{3,2,1...) while((s32[]{:T(128)}, f32[2,128,256]{2,1,0:T(8,128)S(1)}, ...), condition=%wide.region_22.23_spmd.clone, body=%wide.region_20.22_spmd.clone.sunk | while | flops 139837440 | bytes 2366588 | solution.py:111
  167.8 1.9 copy.96
  169.7 5.1 %all_gather.48 = bf16[4,2,128]{2,1,0:T(2,128)(2,1)S(1)} all-gather(bf16[1,2,128]{2,1,0:T(2,128)(2,1)} %get-tuple-element.724), channel_id=1, replica_groups=mesh['sp'=4,'tp'=8] {'sp'}, dimensions={0}, use_global_device_ids=true | all-gather | bytes 2560 | tf_op jit(solution)/shard_map/all_gather | solution.py:34
  174.8 1.3 convolution_convert_fusion.1
  176.1 7.9 %all-gather.2 = bf16[8,128,256]{2,1,0:T(8,128)(2,1)} all-gather(bf16[2,128,256]{2,1,0:T(8,128)(2,1)S(1)} %convolution_convert_fusion.1), channel_id=4, replica_groups=mesh['sp'=4,'tp'=8] {'sp'}, dimensions={0}, use_global_device_ids=true | all-gather | bytes 655360 | tf_op jit(solution)/shard_map/all_gather | solution.py:34
  184.0 4.4 %while.90 = (s32[]{:T(128)}, f32[2,128]{1,0:T(2,128)S(1)}, f32[2,128,256]{2,1,0:T(8,128)S(1)}, s32[]{:T(128)}, bf16[4,2,128]{2,1,0:T(2,128)(2,1)S(1)}, /*index=5...) while((s32[]{:T(128)}, f32[2,128]{1,0:T(2,128)S(1)}, ...), condition=%wide.region_25.26_spmd.clone, body=%wide.region_24.25_spmd.clone.sunk | while | flops 328968 | bytes 660669 | solution.py:52
  188.4 2.4 fusion.46
  190.8 3.1 %rev.38 = f32[128,2,256]{0,2,1:T(8,128)} reverse(f32[128,2,256]{0,2,1:T(8,128)} %fusion.46), dimensions={0} | reverse | bytes 524288 | tf_op jit(solution)/shard_map/jit(_flip)/rev | solution.py:71
  194.0 1.1 broadcast_add_fusion.1
  195.8 4.3 %while.86 = (s32[]{:T(128)}, f32[2,128,256]{2,1,0:T(8,128)S(1)}, f32[2,64,2,256]{3,1,0,2:T(8,128)}, f32[2,64,2,128]{3,2,1,0:T(2,128)S(1)}, f32[2,64,2,128]{3,2,1...) while((s32[]{:T(128)}, f32[2,128,256]{2,1,0:T(8,128)S(1)}, ...), condition=%wide.region_9.10_spmd.clone, body=%wide.region_7.9_spmd.clone.sunk | while | flops 139837440 | bytes 2594944 | solution.py:111
  200.1 1.8 copy.86
  201.9 5.0 %all_gather.42 = bf16[4,2,128]{2,1,0:T(2,128)(2,1)S(1)} all-gather(bf16[1,2,128]{2,1,0:T(2,128)(2,1)S(1)} %get-tuple-element.720), channel_id=1, replica_groups=mesh['sp'=4,'tp'=8] {'sp'}, dimensions={0}, use_global_device_ids=true | all-gather | bytes 2560 | tf_op jit(solution)/shard_map/all_gather | solution.py:34
  207.3 7.6 %all-gather = bf16[8,128,256]{2,1,0:T(8,128)(2,1)S(1)} all-gather(bf16[2,128,256]{2,1,0:T(8,128)(2,1)S(1)} %convolution_convert_fusion.3), channel_id=2, replica_groups=mesh['sp'=4,'tp'=8] {'sp'}, dimensions={0}, use_global_device_ids=true | all-gather | bytes 655360 | tf_op jit(solution)/shard_map/all_gather | solution.py:34
  215.7 1.7 fusion.130
  217.8 1.7 fusion.68
  219.5 35.8 %all-gather.9.cloned.1.call-done = bf16[128,4096]{1,0:T(8,128)(2,1)} async-done(((bf16[128,512]{1,0:T(8,128)(2,1)}), bf16[128,4096]{1,0:T(8,128)(2,1)}) %all-gather.9.cloned.1.call-update) | async-done | bytes 1048592 | tf_op jit(solution)/shard_map/all_gather | solution.py:297
  255.3 4.7 %fusion.50 = bf16[128,512]{1,0:T(8,128)(2,1)} fusion(bf16[128,4096]{1,0:T(8,128)(2,1)} %all-gather.9.cloned.1.call-done, bf16[512,4096]{1,0:T(8,128)(2,1)} %param.45, bf16[128,512]{1,0:T(8,128)(2,1)S(1)} %copy-done.11, f32[512]{0:T(512)S(1)} %bitcast.285), kind=kOutput, calls=%fused_computation.87 | convolution fusion | flops 537133056 | bytes 5507072 | tf_op jit(solution)/shard_map/dot_general | solution.py:56
  (194 shorter events, 40.2 us)
Async XLA Ops:
  6.5 82.4 %copy-start = (bf16[256,4096]{1,0:T(8,128)(2,1)S(1)}, bf16[256,4096]{1,0:T(8,128)(2,1)}, u32[]{:S(2)}) copy-start(bf16[256,4096]{1,0:T(8,128)(2,1)} %param.37) | copy-start | bytes 6291460
  6.5 46.8 %copy-start.17 = (bf16[16,512]{1,0:T(8,128)(2,1)S(1)}, bf16[16,512]{1,0:T(8,128)(2,1)}, u32[]{:S(2)}) copy-start(bf16[16,512]{1,0:T(8,128)(2,1)} %param.30) | copy-start | bytes 49156
  6.5 46.7 %copy-start.16 = (bf16[2,16,2048]{2,1,0:T(8,128)(2,1)S(1)}, bf16[2,16,2048]{2,1,0:T(8,128)(2,1)}, u32[]{:S(2)}) copy-start(bf16[2,16,2048]{2,1,0:T(8,128)(2,1)} %param.41) | copy-start | bytes 393220
  6.5 121.0 %all-gather.7.cloned.1.call-start = ((), (), s32[]{:S(2)}) async-start(), calls=%async_computation | async-start | bytes 1179648 | tf_op jit(solution)/shard_map/all_gather | solution.py:204
  51.4 203.9 %all-gather.9.cloned.1.call-start = ((), (), s32[]{:S(2)}) async-start(), calls=%async_computation.1 | async-start | bytes 1179648 | tf_op jit(solution)/shard_map/all_gather | solution.py:297
  53.3 49.8 %copy-start.15 = (bf16[16,4096]{1,0:T(8,128)(2,1)}, bf16[16,4096]{1,0:T(8,128)(2,1)S(1)}, u32[]{:S(2)}) copy-start(bf16[16,4096]{1,0:T(8,128)(2,1)S(1)} %get-tuple-element.713) | copy-start | bytes 393220
  53.3 49.8 %copy-start.18 = (bf16[1,16,2048]{2,1,0:T(8,128)(2,1)}, bf16[1,16,2048]{2,1,0:T(8,128)(2,1)S(1)}, u32[]{:S(2)}) copy-start(bf16[1,16,2048]{2,1,0:T(8,128)(2,1)S(1)} %get-tuple-element.721) | copy-start | bytes 196612
  53.3 49.8 %copy-start.19 = (bf16[1,16,2048]{2,1,0:T(8,128)(2,1)}, bf16[1,16,2048]{2,1,0:T(8,128)(2,1)S(1)}, u32[]{:S(2)}) copy-start(bf16[1,16,2048]{2,1,0:T(8,128)(2,1)S(1)} %get-tuple-element.722) | copy-start | bytes 196612
  84.4 5.4 %copy-start.22 = (f32[1,256]{1,0:T(1,128)}, f32[1,256]{1,0:T(1,128)S(1)}, u32[]{:S(2)}) copy-start(f32[1,256]{1,0:T(1,128)S(1)} %get-tuple-element.747) | copy-start | bytes 3076
  103.9 0.8 copy-start.3
  126.8 0.7 copy-start.5
  127.5 9.4 %copy-start.1 = (bf16[128,4096]{1,0:T(8,128)(2,1)S(1)}, bf16[128,4096]{1,0:T(8,128)(2,1)}, u32[]{:S(2)}) copy-start(bf16[128,4096]{1,0:T(8,128)(2,1)} %all-gather.7.cloned.1.call-done) | copy-start | bytes 3145732
  152.8 9.1 %copy-start.2 = (f32[2,128,256]{2,1,0:T(8,128)S(1)}, f32[2,128,256]{2,1,0:T(8,128)}, u32[]{:S(2)}) copy-start(f32[2,128,256]{2,1,0:T(8,128)} %custom-call.4) | copy-start | bytes 786436
  161.9 22.1 %copy-start.8 = (f32[2,128,256]{2,1,0:T(8,128)S(1)}, f32[2,128,256]{2,1,0:T(8,128)}, u32[]{:S(2)}) copy-start(f32[2,128,256]{2,1,0:T(8,128)} %custom-call.6) | copy-start | bytes 786436
  167.8 20.6 %copy-start.6 = (f32[2,128,256]{2,1,0:T(8,128)S(1)}, f32[2,128,256]{2,1,0:T(8,128)}, u32[]{:S(2)}) copy-start(f32[2,128,256]{2,1,0:T(8,128)} %copy-done.5) | copy-start | bytes 786436
  167.8 28.0 %copy-start.9 = (f32[2,64,2,256]{3,2,1,0:T(2,128)S(1)}, f32[2,64,2,256]{3,2,1,0:T(2,128)}, u32[]{:S(2)}) copy-start(f32[2,64,2,256]{3,2,1,0:T(2,128)} %reshape_reshape.7) | copy-start | bytes 786436
  176.1 17.8 %copy-start.14 = (f32[128,256]{1,0:T(8,128)S(1)}, f32[128,256]{1,0:T(8,128)}, u32[]{:S(2)}) copy-start(f32[128,256]{1,0:T(8,128)} %broadcast_multiply_fusion) | copy-start | bytes 393220
  176.1 19.7 %copy-start.10 = (f32[2,64,2,128]{3,2,1,0:T(2,128)S(1)}, f32[2,64,2,128]{3,2,1,0:T(2,128)}, u32[]{:S(2)}) copy-start(f32[2,64,2,128]{3,2,1,0:T(2,128)} %reshape_reshape.6) | copy-start | bytes 393220
  195.8 11.2 %copy-start.13 = (f32[128,2,128]{2,1,0:T(2,128)S(1)}, f32[128,2,128]{2,1,0:T(2,128)}, u32[]{:S(2)}) copy-start(f32[128,2,128]{2,1,0:T(2,128)} %get-tuple-element.717) | copy-start | bytes 393220
  195.8 19.2 %copy-start.7 = (f32[2,128,256]{2,1,0:T(8,128)S(1)}, f32[2,128,256]{2,1,0:T(8,128)}, u32[]{:S(2)}) copy-start(f32[2,128,256]{2,1,0:T(8,128)} %custom-call.2) | copy-start | bytes 786436
  200.1 15.6 %copy-start.4 = (f32[2,128,256]{2,1,0:T(8,128)S(1)}, f32[2,128,256]{2,1,0:T(8,128)}, u32[]{:S(2)}) copy-start(f32[2,128,256]{2,1,0:T(8,128)} %copy-done.3) | copy-start | bytes 786436
  200.1 17.7 %copy-start.20 = (f32[512]{0:T(512)S(1)}, f32[512]{0:T(512)}, u32[]{:S(2)}) copy-start(f32[512]{0:T(512)} %param.44) | copy-start | bytes 6148
  207.3 8.4 %copy-start.12 = (f32[128,2,256]{0,2,1:T(8,128)S(1)}, f32[128,2,256]{0,2,1:T(8,128)}, u32[]{:S(2)}) copy-start(f32[128,2,256]{0,2,1:T(8,128)} %rev.38) | copy-start | bytes 786436
  207.3 12.2 %copy-start.21 = (f32[2,512]{1,0:T(2,128)S(1)}, f32[2,512]{1,0:T(2,128)}, u32[]{:S(2)}) copy-start(f32[2,512]{1,0:T(2,128)} %get-tuple-element.705) | copy-start | bytes 12292
  207.3 47.9 %copy-start.11 = (bf16[128,512]{1,0:T(8,128)(2,1)S(1)}, bf16[128,512]{1,0:T(8,128)(2,1)}, u32[]{:S(2)}) copy-start(bf16[128,512]{1,0:T(8,128)(2,1)} %param.29) | copy-start | bytes 393220
Sparse Core Ops, SparseCore 0:
  51.5 35.1 all-gather.6
  219.6 35.6 all-gather.8
where the time goes:
time: 269 us; the launch traced here: 267 us
  blocking collectives  116 us (43%)
  matrix products  46.5 us (17%)
  waiting for transfers between devices  35.8 us (13%)
  other arithmetic  28.5 us (11%)
  local copies, waits for them, and re-layouts  25 us (9%)
  between operations  13.9 us (5%)
    all_gather x1, waiting for transfers between devices, local(): lax.all_gather(heads_out, 'tp', axis=1, tiled=True)  35.8 us
    all_gather x1, blocking collectives, local(): ctx_piece = lax.all_gather(normed_ctx, 'tp', axis=1, tiled=True)  31 us
    dot_general x12, matrix products, linear(): lax.dot_general(rows, weight, (((1,), (1,)), ((), ())), preferred_element...  28.7 us
    all_gather x4, blocking collectives, carried_in(): lax.all_gather(part.astype(kind), axis)  25.6 us
    psum x1, blocking collectives, local(): lax.psum((jnp.sum(lat_f, axis=1, keepdims=True), jnp.sum(lat_f * lat_f, a...  21.7 us
    psum x1, blocking collectives, local(): lax.psum((linear(conds, shift_matrix), linear(conds, scale_matrix), linea...  13.2 us
    all_gather x1, blocking collectives, local(): lax.all_gather(cb_state[None].astype(jnp.bfloat16), 'sp', axis=0, tiled=T...  7.46 us
    all_gather x1, blocking collectives, local(): lax.all_gather(cf_state[None].astype(jnp.bfloat16), 'sp', axis=0, tiled=T...  7.28 us
  transfers between devices with their start and end apart: 2, of which 1 were waited for; matrix products, arithmetic and copies ran while one was open for 7% of the time, Pallas kernels for 0%

commit v1 on v0

--- a/solution.py
+++ b/solution.py
@@ -1,6 +1,10 @@
+import functools
+
 import jax
 import jax.numpy as jnp
 from jax import lax
+from jax.experimental import pallas as pl
+from jax.experimental.pallas import tpu as pltpu
 from jax.sharding import PartitionSpec as P
 
 D = 4096
@@ -9,6 +13,7 @@
 DECAY_RANK = 16
 BLK = 64
 VGROUP = 64
+MESH = pl.DeviceIdType.MESH
 
 
 epsilon = 1e-05
@@ -298,6 +303,539 @@
     return (latent.astype(jnp.float32) + gates[0] * branch).astype(jnp.bfloat16)
 
 
+def exact(a, b):
+    return lax.dot_general(
+        a, b, (((1,), (0,)), ((), ())), precision=precise, preferred_element_type=jnp.float32
+    )
+
+
+def nt(a, b):
+    return lax.dot_general(a, b, (((1,), (1,)), ((), ())), preferred_element_type=jnp.float32)
+
+
+def nn(a, b):
+    return lax.dot_general(a, b, (((1,), (0,)), ((), ())), preferred_element_type=jnp.float32)
+
+
+def tn(a, b):
+    return lax.dot_general(a, b, (((0,), (0,)), ((), ())), preferred_element_type=jnp.float32)
+
+
+def short(value):
+    return value.astype(jnp.bfloat16)
+
+
+def log_decay_of(low, up, bias):
+    pre = exact(low, up) + bias
+    return (jnp.minimum(pre, 0.0) - jnp.log1p(jnp.exp(-jnp.abs(pre)))) / gate_norm
+
+
+def triangle_of(size, upper):
+    i = lax.broadcasted_iota(jnp.int32, (size, size), 0)
+    j = lax.broadcasted_iota(jnp.int32, (size, size), 1)
+    return (j >= i) if upper else (j <= i)
+
+
+def layer_kernel(
+    n,
+    s,
+    rows,
+    crows,
+    feats,
+    heads,
+    dv,
+    latent,
+    context,
+    conditioning,
+    prompt,
+    shift_m,
+    scale_m,
+    gate_m,
+    query_m,
+    key_m,
+    value_m,
+    og_m,
+    down,
+    up,
+    bias,
+    spike,
+    gain,
+    out_m,
+    out_ref,
+    x_all,
+    xn,
+    mod_w,
+    proj_w,
+    out_w,
+    down_v,
+    up_v,
+    bias_v,
+    spike_v,
+    gain_v,
+    cond_v,
+    mod_own,
+    mod_recv,
+    mod_all,
+    proj,
+    ctx_kv,
+    ctx_low,
+    tot_own,
+    tot_recv,
+    st_own,
+    st_recv,
+    local_out,
+    ho_all,
+    load_sem,
+    lat_s,
+    lat_r,
+    ctx_s,
+    ctx_r,
+    m1_s,
+    m1_r,
+    m2_s,
+    m2_r,
+    kv_s,
+    kv_r,
+    lo_s,
+    lo_r,
+    to_s,
+    to_r,
+    st_s,
+    st_r,
+    ho_s,
+    ho_r,
+):
+    me = lax.axis_index("tp")
+    sp = lax.axis_index("sp")
+    hk = heads * DK
+    hv = heads * dv
+    model = n * feats
+    mine = pl.ds(pl.multiple_of(me * feats, feats), feats)
+
+    loads = []
+
+    def load(src, dst):
+        copy = pltpu.make_async_copy(src, dst, load_sem.at[len(loads)])
+        loads.append(copy)
+        copy.start()
+        return copy
+
+    first = [
+        load(conditioning, cond_v.at[0]),
+        load(prompt, cond_v.at[1]),
+        load(shift_m, mod_w.at[0]),
+        load(scale_m, mod_w.at[1]),
+        load(gate_m, mod_w.at[2]),
+    ]
+    own_x = [
+        load(latent, x_all.at[pl.ds(0, rows), mine]),
+        load(context, x_all.at[pl.ds(rows, crows), mine]),
+    ]
+    weights = [
+        load(query_m, proj_w.at[pl.ds(0, hk)]),
+        load(key_m, proj_w.at[pl.ds(hk, hk)]),
+        load(value_m, proj_w.at[pl.ds(2 * hk, hv)]),
+        load(og_m, proj_w.at[pl.ds(2 * hk + hv, hv)]),
+        load(down, down_v),
+    ]
+    head_cols = pl.ds(pl.multiple_of(me * hk, hk), hk)
+    small = [
+        load(up.at[:, :, head_cols], up_v),
+        load(bias.at[:, head_cols], bias_v),
+        load(spike, spike_v),
+        load(gain, gain_v),
+    ]
+    last = load(out_m, out_w)
+
+    barrier = pltpu.get_barrier_semaphore()
+    for d in range(1, n):
+        pl.semaphore_signal(
+            barrier, inc=1, device_id={"tp": lax.rem(me + d, n)}, device_id_type=MESH
+        )
+    for d in range(1, s):
+        pl.semaphore_signal(
+            barrier, inc=1, device_id={"sp": lax.rem(sp + d, s)}, device_id_type=MESH
+        )
+    pl.semaphore_wait(barrier, n - 1 + s - 1)
+
+    started = []
+
+    def send(src, dst, send_sem, recv_sem, axis, d):
+        index, count = (me, n) if axis == "tp" else (sp, s)
+        copy = pltpu.make_async_remote_copy(
+            src_ref=src,
+            dst_ref=dst,
+            send_sem=send_sem.at[d - 1],
+            recv_sem=recv_sem.at[d - 1],
+            device_id={axis: lax.rem(index + d, count)},
+            device_id_type=MESH,
+        )
+        copy.start()
+        started.append(copy)
+        return copy
+
+    lat_copies, ctx_copies = {}, {}
+    for d in range(1, n):
+        lat_copies[d] = send(
+            latent, x_all.at[pl.ds(0, rows), mine], lat_s, lat_r, "tp", d
+        )
+        ctx_copies[d] = send(
+            context, x_all.at[pl.ds(rows, crows), mine], ctx_s, ctx_r, "tp", d
+        )
+
+    for copy in first:
+        copy.wait()
+    row_of = lax.broadcasted_iota(jnp.int32, (16, cond_v.shape[2]), 0)
+    conds = jnp.where(
+        row_of == 0, cond_v[0].astype(jnp.float32), cond_v[1].astype(jnp.float32)
+    )
+    conds = short(conds * lax.logistic(conds))
+    for which in range(3):
+        mod_own[2 * which : 2 * which + 2, :] = nt(conds, mod_w[which])[0:2]
+    mod_own[6:8, :] = jnp.zeros((2, feats), jnp.float32)
+    m1 = {
+        d: send(mod_own, mod_recv.at[d - 1], m1_s, m1_r, "sp", d) for d in range(1, s)
+    }
+
+    for copy in own_x:
+        copy.wait()
+
+    def stats(columns):
+        block = x_all[:, columns].astype(jnp.float32)
+        return jnp.sum(block, axis=1, keepdims=True), jnp.sum(block * block, axis=1, keepdims=True)
+
+    row_sum, row_squares = stats(mine)
+
+    for d in range(1, s):
+        m1[d].wait_recv()
+    total = mod_own[...]
+    for d in range(1, s):
+        total = total + mod_recv[d - 1]
+    mod_all[:, mine] = total
+    m2 = {
+        d: send(mod_all.at[:, mine], mod_all.at[:, mine], m2_s, m2_r, "tp", d)
+        for d in range(1, n)
+    }
+    for d in range(1, n):
+        lat_copies[d].wait_recv()
+        ctx_copies[d].wait_recv()
+        source = lax.rem(me - d + n, n)
+        a, b = stats(pl.ds(pl.multiple_of(source * feats, feats), feats))
+        row_sum, row_squares = row_sum + a, row_squares + b
+    mean = row_sum / model
+    spread = lax.rsqrt(row_squares / model - mean * mean + epsilon)
+    for d in range(1, n):
+        m2[d].wait_recv()
+    for block in range(n):
+        cols = slice(block * feats, (block + 1) * feats)
+        x = (x_all[:, cols].astype(jnp.float32) - mean) * spread
+        mod = mod_all[:, cols]
+        xn[0:rows, cols] = short(x[0:rows] * (1.0 + mod[2:3]) + mod[0:1])
+        xn[rows:, cols] = short(x[rows:] * (1.0 + mod[3:4]) + mod[1:2])
+
+    for copy in weights:
+        copy.wait()
+    tile = min(256, hk)
+
+    def project(t):
+        cols = pl.ds(pl.multiple_of(t * tile, tile), tile)
+        proj[:, cols] = short(nt(xn[...], proj_w[cols, :]))
+
+    def project_range(begin, end):
+        @pl.loop(begin // tile, end // tile)
+        def _(t):
+            project(t)
+
+    project_range(hk, 2 * hk + hv)
+    low = [nn(xn[...], down_v[direction]) for direction in range(2)]
+
+    own_ctx = pl.ds(pl.multiple_of(sp * crows, crows), crows)
+    ctx_kv[own_ctx, :] = proj[rows:, hk : 2 * hk + hv]
+    ctx_low[own_ctx, :] = jnp.zeros((crows, ctx_low.shape[1]), jnp.float32)
+    for direction in range(2):
+        ctx_low[own_ctx, direction * 128 : direction * 128 + DECAY_RANK] = low[direction][rows:]
+    kv = {
+        d: send(ctx_kv.at[own_ctx], ctx_kv.at[own_ctx], kv_s, kv_r, "sp", d)
+        for d in range(1, s)
+    }
+    lo = {
+        d: send(ctx_low.at[own_ctx], ctx_low.at[own_ctx], lo_s, lo_r, "sp", d)
+        for d in range(1, s)
+    }
+
+    for copy in small:
+        copy.wait()
+    head_lane = lax.broadcasted_iota(jnp.int32, (rows, spike_v.shape[2]), 1)
+    ups = [up_v[direction].astype(jnp.float32) for direction in range(2)]
+    cum = []
+    for direction in range(2):
+        logs = log_decay_of(low[direction][0:rows], ups[direction], bias_v[direction : direction + 1])
+        added = [
+            jnp.broadcast_to(
+                jnp.sum(
+                    jnp.where(head_lane == me * heads + h, spike_v[direction], 0.0),
+                    axis=1,
+                    keepdims=True,
+                ),
+                (rows, DK),
+            )
+            for h in range(heads)
+        ]
+        logs = logs + jnp.concatenate(added, axis=1)
+        cum.append(exact(triangle_of(rows, direction == 1).astype(jnp.float32), logs))
+    whole = [cum[0][rows - 1 : rows], cum[1][0:1]]
+    tot_own[0:1, :] = whole[0]
+    tot_own[1:2, :] = whole[1]
+    tot_own[2:8, :] = jnp.zeros((6, hk), jnp.float32)
+    to = {d: send(tot_own, tot_recv.at[d - 1], to_s, to_r, "sp", d) for d in range(1, s)}
+
+    keys = proj[0:rows, hk : 2 * hk].astype(jnp.float32)
+    for direction in range(2):
+        weighted = short(keys * jnp.exp(whole[direction] - cum[direction]))
+        for h in range(heads):
+            st_own[direction, h * DK : (h + 1) * DK, :] = short(
+                tn(
+                    weighted[:, h * DK : (h + 1) * DK],
+                    proj[0:rows, 2 * hk + h * dv : 2 * hk + (h + 1) * dv],
+                )
+            )
+    st = {}
+    for d in range(1, s):
+        later = lax.rem(sp + d, s) > sp
+        st[d] = send(
+            st_own.at[jnp.where(later, 0, 1)], st_recv.at[d - 1], st_s, st_r, "sp", d
+        )
+
+    project_range(0, hk)
+    project_range(2 * hk + hv, 2 * hk + 2 * hv)
+
+    queries = proj[0:rows, 0:hk].astype(jnp.float32) * DK ** (-0.5)
+    blocks = rows // BLK
+
+    def span(b):
+        return slice(b * BLK, (b + 1) * BLK)
+
+    inside = [[], []]
+    for b in range(blocks):
+        f = cum[0][span(b)]
+        inside[0].append(f if b == 0 else f - cum[0][b * BLK - 1 : b * BLK])
+        f = cum[1][span(b)]
+        inside[1].append(
+            f if b == blocks - 1 else f - cum[1][(b + 1) * BLK : (b + 1) * BLK + 1]
+        )
+    ends = [[part[BLK - 1 : BLK] for part in inside[0]], [part[0:1] for part in inside[1]]]
+    q_dec = [[short(queries[span(b)] * jnp.exp(inside[e][b])) for b in range(blocks)] for e in range(2)]
+    k_dec = [[short(keys[span(b)] * jnp.exp(-inside[e][b])) for b in range(blocks)] for e in range(2)]
+    k_end = [
+        [short(keys[span(b)] * jnp.exp(ends[e][b] - inside[e][b])) for b in range(blocks)]
+        for e in range(2)
+    ]
+    lower, upper = triangle_of(BLK, False), triangle_of(BLK, True)
+    for h in range(heads):
+        ch = slice(h * DK, (h + 1) * DK)
+        lines = []
+        for b in range(blocks):
+            line = []
+            for c in range(blocks):
+                if b == c:
+                    line.append(
+                        jnp.where(lower, nt(q_dec[0][b][:, ch], k_dec[0][b][:, ch]), 0.0)
+                        + jnp.where(upper, nt(q_dec[1][b][:, ch], k_dec[1][b][:, ch]), 0.0)
+                    )
+                    continue
+                e = 0 if c < b else 1
+                near = q_dec[e][b][:, ch]
+                between = range(c + 1, b) if c < b else range(b + 1, c)
+                if len(between) > 0:
+                    gap = sum(ends[e][m][:, ch] for m in between)
+                    near = short(queries[span(b)][:, ch] * jnp.exp(inside[e][b][:, ch] + gap))
+                line.append(nt(near, k_end[e][c][:, ch]))
+            lines.append(jnp.concatenate(line, axis=1) if blocks > 1 else line[0])
+        scores = short(jnp.concatenate(lines, axis=0) if blocks > 1 else lines[0])
+        local_out[:, h * dv : (h + 1) * dv] = nn(
+            scores, proj[0:rows, 2 * hk + h * dv : 2 * hk + (h + 1) * dv]
+        )
+
+    for d in range(1, s):
+        kv[d].wait_recv()
+        lo[d].wait_recv()
+    ctx_keys = ctx_kv[:, 0:hk].astype(jnp.float32)
+    ctx_states = []
+    for direction in range(2):
+        logs = log_decay_of(
+            ctx_low[:, direction * 128 : direction * 128 + DECAY_RANK],
+            ups[direction],
+            bias_v[direction : direction + 1],
+        )
+        length = s * crows
+        c = exact(triangle_of(length, direction == 1).astype(jnp.float32), logs)
+        end = c[length - 1 : length] if direction == 0 else c[0:1]
+        weighted = short(ctx_keys * jnp.exp(end - c))
+        ctx_states.append(
+            [
+                short(
+                    tn(
+                        weighted[:, h * DK : (h + 1) * DK],
+                        ctx_kv[:, hk + h * dv : hk + (h + 1) * dv],
+                    )
+                )
+                for h in range(heads)
+            ]
+        )
+
+    for d in range(1, s):
+        to[d].wait_recv()
+    places = {d: lax.rem(sp - d + s, s) for d in range(1, s)}
+
+    def passed(low_end, high_end, direction):
+        result = jnp.zeros((1, hk), jnp.float32)
+        for d in range(1, s):
+            held = jnp.where((places[d] > low_end) & (places[d] < high_end), 1.0, 0.0)
+            result = result + held * tot_recv[d - 1][direction : direction + 1]
+        return result
+
+    ctx_reach = [
+        short(queries * jnp.exp(cum[0] + passed(-1, sp, 0))),
+        short(queries * jnp.exp(cum[1] + passed(sp, s, 1))),
+    ]
+    for h in range(heads):
+        ch = slice(h * DK, (h + 1) * DK)
+        local_out[:, h * dv : (h + 1) * dv] += nn(
+            jnp.concatenate([r[:, ch] for r in ctx_reach], axis=1),
+            jnp.concatenate([ctx_states[e][h] for e in range(2)], axis=0),
+        )
+    reach = []
+    for d in range(1, s):
+        p = places[d]
+        before = jnp.where(p < sp, 1.0, 0.0)
+        exponent = before * (cum[0] + passed(p, sp, 0)) + (1.0 - before) * (
+            cum[1] + passed(sp, p, 1)
+        )
+        reach.append(short(queries * jnp.exp(exponent)))
+    gate_rows = proj[0:rows, 2 * hk + hv :].astype(jnp.float32)
+    small_gate = gate_rows * lax.logistic(gate_rows) * gain_v[...]
+    gi = lax.broadcasted_iota(jnp.int32, (dv, dv), 0) // VGROUP
+    gj = lax.broadcasted_iota(jnp.int32, (dv, dv), 1) // VGROUP
+    group = jnp.where(gi == gj, 1.0, 0.0).astype(jnp.bfloat16)
+    for d in range(1, s):
+        st[d].wait_recv()
+    for h in range(heads):
+        ch = slice(h * DK, (h + 1) * DK)
+        vc = slice(h * dv, (h + 1) * dv)
+        o = local_out[:, vc]
+        for d in range(1, s):
+            o = o + nn(reach[d - 1][:, ch], st_recv[d - 1, ch, :])
+        squares = o * o
+        top = short(squares)
+        rest = short(squares - top.astype(jnp.float32))
+        power = (nn(top, group) + nn(rest, group)) * (1.0 / VGROUP)
+        ho_all[me, :, vc] = short(o * lax.rsqrt(power + epsilon) * small_gate[:, vc])
+
+    ho = {d: send(ho_all.at[me], ho_all.at[me], ho_s, ho_r, "tp", d) for d in range(1, n)}
+    last.wait()
+    branch = nt(ho_all[me], out_w[:, mine])
+    for d in range(1, n):
+        ho[d].wait_recv()
+        source = lax.rem(me - d + n, n)
+        branch = branch + nt(
+            ho_all[source], out_w[:, pl.ds(pl.multiple_of(source * feats, feats), feats)]
+        )
+    gates = mod_all[:, mine][4:5]
+    out_ref[...] = short(x_all[0:rows, mine].astype(jnp.float32) + gates * branch)
+    for copy in started:
+        copy.wait_send()
+
+
+def one_kernel(
+    latent,
+    context,
+    conditioning,
+    context_prompt_vector,
+    shift_matrix,
+    scale_matrix,
+    residual_gate_matrix,
+    query_matrix,
+    key_matrix,
+    value_matrix,
+    gate_matrix,
+    decay_down_factor,
+    decay_up_factor,
+    decay_key_bias,
+    spike_log_decay,
+    output_gain,
+    output_matrix,
+):
+    n, s = lax.axis_size("tp"), lax.axis_size("sp")
+    rows, feats = latent.shape
+    crows = context.shape[0]
+    heads = HEADS // n
+    hk, hv = query_matrix.shape[0], value_matrix.shape[0]
+    dv = hv // heads
+    model = n * feats
+    both = rows + crows
+    inputs = conditioning.shape[0]
+    bf, f32 = jnp.bfloat16, jnp.float32
+    vmem, dma = pltpu.VMEM, pltpu.SemaphoreType.DMA
+    pair = lambda k: [dma((k,)), dma((k,))]
+    scratch = [
+        vmem((both, model), bf),
+        vmem((both, model), bf),
+        vmem((3, feats, inputs), bf),
+        vmem((2 * hk + 2 * hv, model), bf),
+        vmem((output_matrix.shape[0], model), bf),
+        vmem((2, model, DECAY_RANK), bf),
+        vmem((2, DECAY_RANK, hk), bf),
+        vmem((2, hk), f32),
+        vmem(spike_log_decay.shape, f32),
+        vmem((1, hv), f32),
+        vmem((2, 1, inputs), bf),
+        vmem((8, feats), f32),
+        vmem((s - 1, 8, feats), f32),
+        vmem((8, model), f32),
+        vmem((both, 2 * hk + 2 * hv), bf),
+        vmem((s * crows, hk + hv), bf),
+        vmem((s * crows, 256), f32),
+        vmem((8, hk), f32),
+        vmem((s - 1, 8, hk), f32),
+        vmem((2, hk, dv), bf),
+        vmem((s - 1, hk, dv), bf),
+        vmem((rows, hv), f32),
+        vmem((n, rows, hv), bf),
+        dma((17,)),
+    ]
+    for count in (n - 1, n - 1, s - 1, n - 1, s - 1, s - 1, s - 1, s - 1, n - 1):
+        scratch += pair(count)
+    return pl.pallas_call(
+        functools.partial(layer_kernel, n, s, rows, crows, feats, heads, dv),
+        out_shape=jax.ShapeDtypeStruct((rows, feats), bf),
+        in_specs=[pl.BlockSpec(memory_space=pl.ANY)] * 17,
+        out_specs=pl.BlockSpec(memory_space=pltpu.VMEM),
+        scratch_shapes=scratch,
+        compiler_params=pltpu.CompilerParams(
+            collective_id=0, has_side_effects=True, vmem_limit_bytes=60 * 1024 * 1024
+        ),
+        name="layer",
+    )(
+        latent,
+        context,
+        conditioning.reshape(1, -1),
+        context_prompt_vector.reshape(1, -1),
+        shift_matrix,
+        scale_matrix,
+        residual_gate_matrix,
+        query_matrix,
+        key_matrix,
+        value_matrix,
+        gate_matrix,
+        decay_down_factor,
+        decay_up_factor,
+        decay_key_bias,
+        spike_log_decay,
+        output_gain.reshape(1, -1),
+        output_matrix,
+    )
+
+
 def solution(mesh):
     placed = (
         P("sp", "tp"),
@@ -318,6 +856,7 @@
         P("tp"),
         P("tp", None),
     )
+    whole_heads = HEADS % mesh.shape["tp"] == 0
     return jax.shard_map(
-        local, mesh=mesh, in_specs=placed, out_specs=P("sp", "tp"), check_vma=False
-    )
+        one_kernel if whole_heads else local, mesh=mesh, in_specs=placed, out_specs=P("sp", "tp"), check_vma=False
+    )

time: 269 us -> 80.6 us (0.30)
  the two profiles are of different devices: /device:TPU:0 before, /device:TPU:29 now
where the time goes in v1:
time: 80.6 us; the launch traced here: 80.3 us
  Pallas kernels  72.1 us (89%)
  local copies, waits for them, and re-layouts  8.23 us (10%)
    pallas_call x1, Pallas kernels, one_kernel(): pl.pallas_call(functools.partial(layer_kernel, n, s, rows, crows, feats,...  72.1 us
    unnamed x3, local copies, waits for them, and re-layouts  5.68 us

profile of v1, /device:TPU:29, one launch (start us, length us, event | category | flops | bytes accessed | tf_op | source)
XLA Modules:
  0.0 80.3 jit_solution(13098165597464811751)
XLA Ops:
  0.0 1.3 %reshape.9.conditioning = bf16[1,1024]{1,0:T(2,128)(2,1)} reshape(bf16[1024]{0:T(1024)(128)(2,1)} %param.19) | data formatting | bytes 4096 | tf_op jit(solution)/shard_map/reshape | solution.py:821
  1.3 1.3 %reshape.10.prompt = bf16[1,1024]{1,0:T(2,128)(2,1)} reshape(bf16[1024]{0:T(1024)(128)(2,1)} %param.20) | data formatting | bytes 4096 | tf_op jit(solution)/shard_map/reshape | solution.py:822
  2.6 1.5 %copy.19.spike = f32[2,128,16]{2,1,0:T(8,128)} copy(f32[2,128,16]{1,2,0:T(8,128)} %param.31) | data formatting | bytes 32768 | tf_op args[14]
  4.0 2.6 %copy.18.down = bf16[2,4096,16]{2,1,0:T(8,128)(2,1)} copy(bf16[2,4096,16]{1,2,0:T(8,128)(2,1)} %param.28) | data formatting | bytes 524288 | tf_op args[11]
  6.7 72.1 %layer.1 = bf16[128,512]{1,0:T(8,128)(2,1)} custom-call(bf16[128,512]{1,0:T(8,128)(2,1)} %latent.1, bf16[16,512]{1,0:T(8,128)(2,1)} %context.1, bf16[1,1024]{1,0:T(2,128)(2,1)} %reshape.9.conditioning, bf16[1,1024]{1,0:T(2,128)(2,1)} %reshape.10.prompt, bf16[512,1024]{1,0:T(8,128)(2,1)} %shift_m.1, bf16[512,1024]{1,0:T(8,128)(2,1)} %scale_m.1, ...), custom_call_target="tpu_custom_call" | custom-call | tf_op jit(solution)/shard_map/layer/pallas_call | solution.py:808
  78.8 1.6 %copy.21 = bf16[128,512]{1,0:T(8,128)(2,1)} copy(bf16[128,512]{1,0:T(8,128)(2,1)} %layer.1) | data formatting | bytes 262144

commit v2 on v1

--- a/solution.py
+++ b/solution.py
@@ -339,6 +339,7 @@
 def layer_kernel(
     n,
     s,
+    inner,
     rows,
     crows,
     feats,
@@ -364,6 +365,8 @@
     out_ref,
     x_all,
     xn,
+    acc,
+    low_acc,
     mod_w,
     proj_w,
     out_w,
@@ -386,10 +389,12 @@
     local_out,
     ho_all,
     load_sem,
-    lat_s,
-    lat_r,
-    ctx_s,
-    ctx_r,
+    xs_up,
+    xr_up,
+    xs_dn,
+    xr_dn,
+    xs_y,
+    xr_y,
     m1_s,
     m1_r,
     m2_s,
@@ -402,8 +407,12 @@
     to_r,
     st_s,
     st_r,
-    ho_s,
-    ho_r,
+    hs_up,
+    hr_up,
+    hs_dn,
+    hr_dn,
+    hs_y,
+    hr_y,
 ):
     me = lax.axis_index("tp")
     sp = lax.axis_index("sp")
@@ -474,21 +483,102 @@
         started.append(copy)
         return copy
 
-    lat_copies, ctx_copies = {}, {}
-    for d in range(1, n):
-        lat_copies[d] = send(
-            latent, x_all.at[pl.ds(0, rows), mine], lat_s, lat_r, "tp", d
-        )
-        ctx_copies[d] = send(
-            context, x_all.at[pl.ds(rows, crows), mine], ctx_s, ctx_r, "tp", d
-        )
+    line = n // inner
+    z, y = lax.div(me, inner), lax.rem(me, inner)
+
+    def block_of(at, column):
+        return at * inner + column
+
+    class Gather:
+        def __init__(self, view, pieces, up, down, across):
+            self.view, self.pieces = view, pieces
+            self.lanes = {"up": up, "down": down, "across": across}
+
+        def copy(self, lane, block, piece, slot, target):
+            sends, recvs = self.lanes[lane]
+            ref = self.view(block, piece)
+            return pltpu.make_async_remote_copy(
+                src_ref=ref,
+                dst_ref=ref,
+                send_sem=sends.at[slot, piece],
+                recv_sem=recvs.at[slot, piece],
+                device_id={"tp": target},
+                device_id_type=MESH,
+            )
+
+        def hop(self, lane, at, piece, slot):
+            target = {
+                "up": block_of(jnp.minimum(z + 1, line - 1), y),
+                "down": block_of(jnp.maximum(z - 1, 0), y),
+                "across": block_of(z, inner - 1 - y),
+            }[lane]
+            return self.copy(lane, block_of(at, y), piece, slot, target)
+
+        def sends(self, k, piece, act):
+            for lane, at, has, onward, slot in (
+                ("up", z - k, z >= k, z + 1 < line, max(2 * k - 1, 0)),
+                ("down", z + k, z + k < line, z > 0, 2 * k),
+            ):
+                if k < line - 1:
+                    pl.when(has & onward)(lambda: act(self.hop(lane, at, piece, k)))
+                if inner > 1 and (k > 0 or lane == "up"):
+                    pl.when(has)(lambda: act(self.hop("across", at, piece, slot)))
+
+        def start(self):
+            for piece in range(self.pieces):
+                self.sends(0, piece, lambda c: c.start())
+
+        def step(self, k):
+            for piece in range(self.pieces):
+                for lane, at, has in (("up", z - k, z >= k), ("down", z + k, z + k < line)):
+                    pl.when(has)(lambda: self.hop(lane, at, piece, k - 1).wait_recv())
+                self.sends(k, piece, lambda c: c.start())
+
+        def column(self, k, work):
+            pl.when(z >= k)(lambda: work(block_of(z - k, y)))
+            pl.when(z + k < line)(lambda: work(block_of(z + k, y)))
+
+        def other(self, k, work):
+            if inner == 1:
+                return
+
+            def arrive(at, slot):
+                block = block_of(at, inner - 1 - y)
+                for piece in range(self.pieces):
+                    self.copy("across", block, piece, slot, block).wait_recv()
+                work(block)
+
+            if k == 0:
+                arrive(z, 0)
+                return
+            pl.when(z >= k)(lambda: arrive(z - k, 2 * k - 1))
+            pl.when(z + k < line)(lambda: arrive(z + k, 2 * k))
+
+        def drain(self):
+            for k in range(line):
+                for piece in range(self.pieces):
+                    self.sends(k, piece, lambda c: c.wait_send())
+
+    both = rows + crows
+    cut = both // 32 * 16
+
+    def x_view(block, piece):
+        part = pl.ds(0, cut) if piece == 0 else pl.ds(cut, both - cut)
+        return x_all.at[part, pl.ds(pl.multiple_of(block * feats, feats), feats)]
+
+    xg = Gather(x_view, 2, (xs_up, xr_up), (xs_dn, xr_dn), (xs_y, xr_y))
+    for copy in own_x:
+        copy.wait()
+    xg.start()
 
     for copy in first:
         copy.wait()
-    row_of = lax.broadcasted_iota(jnp.int32, (16, cond_v.shape[2]), 0)
-    conds = jnp.where(
-        row_of == 0, cond_v[0].astype(jnp.float32), cond_v[1].astype(jnp.float32)
-    )
+    def one_row(which):
+        part = cond_v[which].astype(jnp.float32)
+        return jnp.concatenate([part[r : r + 1] for r in range(part.shape[0])], axis=1)
+
+    row_of = lax.broadcasted_iota(jnp.int32, (16, shift_m.shape[1]), 0)
+    conds = jnp.where(row_of == 0, one_row(0), one_row(1))
     conds = short(conds * lax.logistic(conds))
     for which in range(3):
         mod_own[2 * which : 2 * which + 2, :] = nt(conds, mod_w[which])[0:2]
@@ -497,63 +587,83 @@
         d: send(mod_own, mod_recv.at[d - 1], m1_s, m1_r, "sp", d) for d in range(1, s)
     }
 
-    for copy in own_x:
-        copy.wait()
-
-    def stats(columns):
-        block = x_all[:, columns].astype(jnp.float32)
-        return jnp.sum(block, axis=1, keepdims=True), jnp.sum(block * block, axis=1, keepdims=True)
-
-    row_sum, row_squares = stats(mine)
-
+    own = x_all[:, mine]
+    ones = jnp.ones((16, feats), jnp.bfloat16)
+    own_f = own.astype(jnp.float32)
+    rest = own_f * own_f
+    row_squares = jnp.zeros((16, both), jnp.float32)
+    for _ in range(3):
+        top = short(rest)
+        row_squares = row_squares + nt(ones, top)
+        rest = rest - top.astype(jnp.float32)
+    row_sum = nt(ones, own)
+
+    if line > 1:
+        xg.step(1)
     for d in range(1, s):
         m1[d].wait_recv()
     total = mod_own[...]
     for d in range(1, s):
         total = total + mod_recv[d - 1]
     mod_all[:, mine] = total
+    stat_cols = pl.ds(pl.multiple_of(me * feats, feats), both)
+    mod_all[6:7, stat_cols] = row_sum[0:1]
+    mod_all[7:8, stat_cols] = row_squares[0:1]
     m2 = {
         d: send(mod_all.at[:, mine], mod_all.at[:, mine], m2_s, m2_r, "tp", d)
         for d in range(1, n)
     }
-    for d in range(1, n):
-        lat_copies[d].wait_recv()
-        ctx_copies[d].wait_recv()
-        source = lax.rem(me - d + n, n)
-        a, b = stats(pl.ds(pl.multiple_of(source * feats, feats), feats))
-        row_sum, row_squares = row_sum + a, row_squares + b
-    mean = row_sum / model
-    spread = lax.rsqrt(row_squares / model - mean * mean + epsilon)
-    for d in range(1, n):
-        m2[d].wait_recv()
-    for block in range(n):
-        cols = slice(block * feats, (block + 1) * feats)
+    tile = min(256, hk)
+    columns = acc.shape[1]
+    acc[...] = jnp.zeros(acc.shape, jnp.float32)
+    low_acc[...] = jnp.zeros(low_acc.shape, jnp.float32)
+
+    def moments():
+        for d in range(1, n):
+            m2[d].wait_recv()
+        diagonal = lax.broadcasted_iota(jnp.int32, (both, both), 0) == lax.broadcasted_iota(
+            jnp.int32, (both, both), 1
+        )
+
+        def column_of(row):
+            whole_row = sum(mod_all[row : row + 1, b * feats : b * feats + both] for b in range(n))
+            return jnp.sum(jnp.where(diagonal, whole_row, 0.0), axis=1, keepdims=True) / model
+
+        mean = column_of(6)
+        return mean, lax.rsqrt(column_of(7) - mean * mean + epsilon)
+
+    def project_block(block, mean, spread):
+        cols = pl.ds(pl.multiple_of(block * feats, feats), feats)
         x = (x_all[:, cols].astype(jnp.float32) - mean) * spread
         mod = mod_all[:, cols]
-        xn[0:rows, cols] = short(x[0:rows] * (1.0 + mod[2:3]) + mod[0:1])
-        xn[rows:, cols] = short(x[rows:] * (1.0 + mod[3:4]) + mod[1:2])
-
-    for copy in weights:
-        copy.wait()
-    tile = min(256, hk)
-
-    def project(t):
-        cols = pl.ds(pl.multiple_of(t * tile, tile), tile)
-        proj[:, cols] = short(nt(xn[...], proj_w[cols, :]))
-
-    def project_range(begin, end):
-        @pl.loop(begin // tile, end // tile)
+        xn[0:rows, :] = short(x[0:rows] * (1.0 + mod[2:3]) + mod[0:1])
+        xn[rows:, :] = short(x[rows:] * (1.0 + mod[3:4]) + mod[1:2])
+        low_acc[...] += nt(xn[...], down_v[:, cols])
+
+        @pl.loop(0, columns // tile)
         def _(t):
-            project(t)
-
-    project_range(hk, 2 * hk + hv)
-    low = [nn(xn[...], down_v[direction]) for direction in range(2)]
+            out = pl.ds(pl.multiple_of(t * tile, tile), tile)
+            acc[:, out] += nt(xn[...], proj_w[out, cols])
+
+    ready = None
+    for k in range(2, line + 1):
+        if k < line:
+            xg.step(k)
+        if ready is None:
+            ready = moments()
+            for copy in weights:
+                copy.wait()
+            work = lambda block: project_block(block, *ready)
+            work(me)
+        xg.column(k - 1, work)
+        xg.other(k - 2, work)
+    xg.other(line - 1, work)
+    proj[...] = short(acc[...])
 
     own_ctx = pl.ds(pl.multiple_of(sp * crows, crows), crows)
     ctx_kv[own_ctx, :] = proj[rows:, hk : 2 * hk + hv]
     ctx_low[own_ctx, :] = jnp.zeros((crows, ctx_low.shape[1]), jnp.float32)
-    for direction in range(2):
-        ctx_low[own_ctx, direction * 128 : direction * 128 + DECAY_RANK] = low[direction][rows:]
+    ctx_low[own_ctx, 0 : 2 * DECAY_RANK] = low_acc[rows:]
     kv = {
         d: send(ctx_kv.at[own_ctx], ctx_kv.at[own_ctx], kv_s, kv_r, "sp", d)
         for d in range(1, s)
@@ -565,23 +675,24 @@
 
     for copy in small:
         copy.wait()
-    head_lane = lax.broadcasted_iota(jnp.int32, (rows, spike_v.shape[2]), 1)
-    ups = [up_v[direction].astype(jnp.float32) for direction in range(2)]
+    slot_head = lax.broadcasted_iota(jnp.int32, (spike_v.shape[1], hk), 0)
+    lane_head = lax.broadcasted_iota(jnp.int32, (spike_v.shape[1], hk), 1) // DK
+    pick = jnp.where(slot_head == me * heads + lane_head, 1.0, 0.0)
+    none = jnp.zeros((DECAY_RANK, hk), jnp.float32)
+    ups = [
+        jnp.concatenate([up_v[0].astype(jnp.float32), none], axis=0),
+        jnp.concatenate([none, up_v[1].astype(jnp.float32)], axis=0),
+    ]
     cum = []
     for direction in range(2):
-        logs = log_decay_of(low[direction][0:rows], ups[direction], bias_v[direction : direction + 1])
-        added = [
-            jnp.broadcast_to(
-                jnp.sum(
-                    jnp.where(head_lane == me * heads + h, spike_v[direction], 0.0),
-                    axis=1,
-                    keepdims=True,
-                ),
-                (rows, DK),
-            )
-            for h in range(heads)
-        ]
-        logs = logs + jnp.concatenate(added, axis=1)
+        logs = log_decay_of(low_acc[0:rows], ups[direction], bias_v[direction : direction + 1])
+        logs = logs + lax.dot_general(
+            spike_v[direction],
+            pick,
+            (((0,), (0,)), ((), ())),
+            precision=precise,
+            preferred_element_type=jnp.float32,
+        )
         cum.append(exact(triangle_of(rows, direction == 1).astype(jnp.float32), logs))
     whole = [cum[0][rows - 1 : rows], cum[1][0:1]]
     tot_own[0:1, :] = whole[0]
@@ -606,9 +717,6 @@
             st_own.at[jnp.where(later, 0, 1)], st_recv.at[d - 1], st_s, st_r, "sp", d
         )
 
-    project_range(0, hk)
-    project_range(2 * hk + hv, 2 * hk + 2 * hv)
-
     queries = proj[0:rows, 0:hk].astype(jnp.float32) * DK ** (-0.5)
     blocks = rows // BLK
 
@@ -635,10 +743,10 @@
         ch = slice(h * DK, (h + 1) * DK)
         lines = []
         for b in range(blocks):
-            line = []
+            strip = []
             for c in range(blocks):
                 if b == c:
-                    line.append(
+                    strip.append(
                         jnp.where(lower, nt(q_dec[0][b][:, ch], k_dec[0][b][:, ch]), 0.0)
                         + jnp.where(upper, nt(q_dec[1][b][:, ch], k_dec[1][b][:, ch]), 0.0)
                     )
@@ -649,8 +757,8 @@
                 if len(between) > 0:
                     gap = sum(ends[e][m][:, ch] for m in between)
                     near = short(queries[span(b)][:, ch] * jnp.exp(inside[e][b][:, ch] + gap))
-                line.append(nt(near, k_end[e][c][:, ch]))
-            lines.append(jnp.concatenate(line, axis=1) if blocks > 1 else line[0])
+                strip.append(nt(near, k_end[e][c][:, ch]))
+            lines.append(jnp.concatenate(strip, axis=1) if blocks > 1 else strip[0])
         scores = short(jnp.concatenate(lines, axis=0) if blocks > 1 else lines[0])
         local_out[:, h * dv : (h + 1) * dv] = nn(
             scores, proj[0:rows, 2 * hk + h * dv : 2 * hk + (h + 1) * dv]
@@ -663,7 +771,7 @@
     ctx_states = []
     for direction in range(2):
         logs = log_decay_of(
-            ctx_low[:, direction * 128 : direction * 128 + DECAY_RANK],
+            ctx_low[:, 0 : 2 * DECAY_RANK],
             ups[direction],
             bias_v[direction : direction + 1],
         )
@@ -731,19 +839,29 @@
         power = (nn(top, group) + nn(rest, group)) * (1.0 / VGROUP)
         ho_all[me, :, vc] = short(o * lax.rsqrt(power + epsilon) * small_gate[:, vc])
 
-    ho = {d: send(ho_all.at[me], ho_all.at[me], ho_s, ho_r, "tp", d) for d in range(1, n)}
+    def ho_view(block, piece):
+        return ho_all.at[block, pl.ds(piece * (rows // 2), rows // 2)]
+
+    hg = Gather(ho_view, 2, (hs_up, hr_up), (hs_dn, hr_dn), (hs_y, hr_y))
+    hg.start()
     last.wait()
-    branch = nt(ho_all[me], out_w[:, mine])
-    for d in range(1, n):
-        ho[d].wait_recv()
-        source = lax.rem(me - d + n, n)
-        branch = branch + nt(
-            ho_all[source], out_w[:, pl.ds(pl.multiple_of(source * feats, feats), feats)]
-        )
+    local_out[...] = nt(ho_all[me], out_w[:, mine])
+
+    def add_block(block):
+        cols = pl.ds(pl.multiple_of(block * feats, feats), feats)
+        local_out[...] += nt(ho_all[block], out_w[:, cols])
+
+    for k in range(1, line):
+        hg.step(k)
+        hg.other(k - 1, add_block)
+        hg.column(k, add_block)
+    hg.other(line - 1, add_block)
     gates = mod_all[:, mine][4:5]
-    out_ref[...] = short(x_all[0:rows, mine].astype(jnp.float32) + gates * branch)
+    out_ref[...] = short(x_all[0:rows, mine].astype(jnp.float32) + gates * local_out[...])
     for copy in started:
         copy.wait_send()
+    xg.drain()
+    hg.drain()
 
 
 def one_kernel(
@@ -779,22 +897,24 @@
     pair = lambda k: [dma((k,)), dma((k,))]
     scratch = [
         vmem((both, model), bf),
-        vmem((both, model), bf),
+        vmem((both, feats), bf),
+        vmem((both, 2 * hk + 2 * hv), f32),
+        vmem((both, 2 * DECAY_RANK), f32),
         vmem((3, feats, inputs), bf),
         vmem((2 * hk + 2 * hv, model), bf),
         vmem((output_matrix.shape[0], model), bf),
-        vmem((2, model, DECAY_RANK), bf),
+        vmem((2 * DECAY_RANK, model), bf),
         vmem((2, DECAY_RANK, hk), bf),
         vmem((2, hk), f32),
-        vmem(spike_log_decay.shape, f32),
+        vmem((2, HEADS, rows), f32),
         vmem((1, hv), f32),
-        vmem((2, 1, inputs), bf),
+        vmem((2, inputs // 128, 128), bf),
         vmem((8, feats), f32),
         vmem((s - 1, 8, feats), f32),
         vmem((8, model), f32),
         vmem((both, 2 * hk + 2 * hv), bf),
         vmem((s * crows, hk + hv), bf),
-        vmem((s * crows, 256), f32),
+        vmem((s * crows, 128), f32),
         vmem((8, hk), f32),
         vmem((s - 1, 8, hk), f32),
         vmem((2, hk, dv), bf),
@@ -803,10 +923,16 @@
         vmem((n, rows, hv), bf),
         dma((17,)),
     ]
-    for count in (n - 1, n - 1, s - 1, n - 1, s - 1, s - 1, s - 1, s - 1, n - 1):
+    inner = 2 if n % 2 == 0 else 1
+    line = n // inner
+    hops = max(line - 1, 1)
+    lanes = [dma((k, 2)) for k in (hops, hops, hops, hops, 2 * line - 1, 2 * line - 1)]
+    scratch += lanes
+    for count in (s - 1, n - 1, s - 1, s - 1, s - 1, s - 1):
         scratch += pair(count)
+    scratch += lanes
     return pl.pallas_call(
-        functools.partial(layer_kernel, n, s, rows, crows, feats, heads, dv),
+        functools.partial(layer_kernel, n, s, inner, rows, crows, feats, heads, dv),
         out_shape=jax.ShapeDtypeStruct((rows, feats), bf),
         in_specs=[pl.BlockSpec(memory_space=pl.ANY)] * 17,
         out_specs=pl.BlockSpec(memory_space=pltpu.VMEM),
@@ -818,8 +944,8 @@
     )(
         latent,
         context,
-        conditioning.reshape(1, -1),
-        context_prompt_vector.reshape(1, -1),
+        conditioning.reshape(-1, 128),
+        context_prompt_vector.reshape(-1, 128),
         shift_matrix,
         scale_matrix,
         residual_gate_matrix,
@@ -827,10 +953,10 @@
         key_matrix,
         value_matrix,
         gate_matrix,
-        decay_down_factor,
+        jnp.swapaxes(decay_down_factor, 1, 2).reshape(2 * DECAY_RANK, model),
         decay_up_factor,
         decay_key_bias,
-        spike_log_decay,
+        jnp.swapaxes(spike_log_decay, 1, 2),
         output_gain.reshape(1, -1),
         output_matrix,
     )

time: 80.6 us -> 59 us (0.73)
  the two profiles are of different devices: /device:TPU:29 before, /device:TPU:0 now
where the time goes in v2:
time: 59 us; the launch traced here: 58.8 us
  Pallas kernels  57.2 us (97%)
  local copies, waits for them, and re-layouts  1.57 us (3%)
    pallas_call x1, Pallas kernels, one_kernel(): pl.pallas_call(functools.partial(layer_kernel, n, s, inner, rows, crows,...  57.2 us
    unnamed x1, local copies, waits for them, and re-layouts  1.57 us

profile of v2, /device:TPU:0, one launch (start us, length us, event | category | flops | bytes accessed | tf_op | source)
XLA Modules:
  0.0 58.8 jit_solution(10965667156722748990)
XLA Ops:
  0.0 57.2 %layer.1 = bf16[128,512]{1,0:T(8,128)(2,1)} custom-call(bf16[128,512]{1,0:T(8,128)(2,1)} %latent.1, bf16[16,512]{1,0:T(8,128)(2,1)} %context.1, bf16[8,128]{1,0:T(8,128)(2,1)} %bitcast.9, bf16[8,128]{1,0:T(8,128)(2,1)} %bitcast.10, bf16[512,1024]{1,0:T(8,128)(2,1)} %shift_m.1, bf16[512,1024]{1,0:T(8,128)(2,1)} %scale_m.1, bf16[512,1024]{1,0:T(8,128)(2,1)} %gate_m.1, ...), custom_call_target="tpu_custom_call" | custom-call | tf_op jit(solution)/shard_map/layer/pallas_call | solution.py:934
  57.3 1.6 %copy.19 = bf16[128,512]{1,0:T(8,128)(2,1)} copy(bf16[128,512]{1,0:T(8,128)(2,1)} %layer.1) | data formatting | bytes 262144

commit v3 on v2

--- a/solution.py
+++ b/solution.py
@@ -1,4 +1,5 @@
 import functools
+import math
 
 import jax
 import jax.numpy as jnp
@@ -613,7 +614,7 @@
         d: send(mod_all.at[:, mine], mod_all.at[:, mine], m2_s, m2_r, "tp", d)
         for d in range(1, n)
     }
-    tile = min(256, hk)
+    tile = math.gcd(2 * hk + 2 * hv, 512)
     columns = acc.shape[1]
     acc[...] = jnp.zeros(acc.shape, jnp.float32)
     low_acc[...] = jnp.zeros(low_acc.shape, jnp.float32)
@@ -640,9 +641,8 @@
         xn[rows:, :] = short(x[rows:] * (1.0 + mod[3:4]) + mod[1:2])
         low_acc[...] += nt(xn[...], down_v[:, cols])
 
-        @pl.loop(0, columns // tile)
-        def _(t):
-            out = pl.ds(pl.multiple_of(t * tile, tile), tile)
+        for t in range(columns // tile):
+            out = slice(t * tile, (t + 1) * tile)
             acc[:, out] += nt(xn[...], proj_w[out, cols])
 
     ready = None
@@ -840,9 +840,9 @@
         ho_all[me, :, vc] = short(o * lax.rsqrt(power + epsilon) * small_gate[:, vc])
 
     def ho_view(block, piece):
-        return ho_all.at[block, pl.ds(piece * (rows // 2), rows // 2)]
-
-    hg = Gather(ho_view, 2, (hs_up, hr_up), (hs_dn, hr_dn), (hs_y, hr_y))
+        return ho_all.at[block, pl.ds(piece * (rows // 4), rows // 4)]
+
+    hg = Gather(ho_view, 4, (hs_up, hr_up), (hs_dn, hr_dn), (hs_y, hr_y))
     hg.start()
     last.wait()
     local_out[...] = nt(ho_all[me], out_w[:, mine])
@@ -926,11 +926,11 @@
     inner = 2 if n % 2 == 0 else 1
     line = n // inner
     hops = max(line - 1, 1)
-    lanes = [dma((k, 2)) for k in (hops, hops, hops, hops, 2 * line - 1, 2 * line - 1)]
-    scratch += lanes
+    counts = (hops, hops, hops, hops, 2 * line - 1, 2 * line - 1)
+    scratch += [dma((k, 2)) for k in counts]
     for count in (s - 1, n - 1, s - 1, s - 1, s - 1, s - 1):
         scratch += pair(count)
-    scratch += lanes
+    scratch += [dma((k, 4)) for k in counts]
     return pl.pallas_call(
         functools.partial(layer_kernel, n, s, inner, rows, crows, feats, heads, dv),
         out_shape=jax.ShapeDtypeStruct((rows, feats), bf),

time: 59 us -> 50.8 us (0.86)
  Pallas kernels: 57.2 us -> 49 us
    pallas_call x1, Pallas kernels: 57.2 us -> 49 us  [one_kernel(): pl.pallas_call(functools.partial(layer_kernel, n, s, inner, rows, crows,...]
where the time goes in v3:
time: 50.8 us; the launch traced here: 50.6 us
  Pallas kernels  49 us (96%)
  local copies, waits for them, and re-layouts  1.57 us (3%)
    pallas_call x1, Pallas kernels, one_kernel(): pl.pallas_call(functools.partial(layer_kernel, n, s, inner, rows, crows,...  49 us
    unnamed x1, local copies, waits for them, and re-layouts  1.57 us

profile of v3, /device:TPU:0, one launch (start us, length us, event | category | flops | bytes accessed | tf_op | source)
XLA Modules:
  0.0 50.6 jit_solution(3516350239920724735)
XLA Ops:
  0.0 49.0 %layer.1 = bf16[128,512]{1,0:T(8,128)(2,1)} custom-call(bf16[128,512]{1,0:T(8,128)(2,1)} %latent.1, bf16[16,512]{1,0:T(8,128)(2,1)} %context.1, bf16[8,128]{1,0:T(8,128)(2,1)} %bitcast.9, bf16[8,128]{1,0:T(8,128)(2,1)} %bitcast.10, bf16[512,1024]{1,0:T(8,128)(2,1)} %shift_m.1, bf16[512,1024]{1,0:T(8,128)(2,1)} %scale_m.1, bf16[512,1024]{1,0:T(8,128)(2,1)} %gate_m.1, ...), custom_call_target="tpu_custom_call" | custom-call | tf_op jit(solution)/shard_map/layer/pallas_call | solution.py:934
  49.0 1.6 %copy.19 = bf16[128,512]{1,0:T(8,128)(2,1)} copy(bf16[128,512]{1,0:T(8,128)(2,1)} %layer.1) | data formatting | bytes 262144
